TPU v7x, 32 devices: a whole 2x2x4 slice. The times are simulated.
32 devices in a mesh: grp: 2 (over y), sp: 4 (over z), tp: 4 (over x, core).
Axes of the slice: x: 2, y: 2, z: 4, core: 2. Of those that a mesh axis runs over, the one named last changes fastest.
Arguments:
- tokens: bfloat16 [2, 2048, 2048], P('grp', ('sp', 'tp')), parts along dimension 0, may hold values from -6 to 6
- norm_gain: bfloat16 [2048], replicated, may hold values from 0.099609375 to 1.8984375
- w_query: bfloat16 [2048, 1024], P('sp'), may hold values from -0.125 to 0.125
- w_forget: bfloat16 [2048, 1024], P('sp'), may hold values from -0.125 to 0.125
- w_input: bfloat16 [2048, 1024], P('sp'), may hold values from -0.125 to 0.125
- floor_gap: float32 [1024], replicated, may hold values from 0.000146484375 to 0.12
- extra_decay: float32 [2, 2048, 16], P('grp', ('sp', 'tp')), parts along dimension 0, may hold values from -1.4 to 0, as said below
- init_state: float32 [2, 16, 64, 64], P('grp'), parts along dimension 0, may hold values from -0.078125 to 0.078125
- head_norm_gain: bfloat16 [1024], replicated, may hold values from 0.099609375 to 1.8984375
- w_output: bfloat16 [1024, 2048], P(None, 'sp'), may hold values from -0.1875 to 0.1875
Outputs:
- mixed: bfloat16 [2, 2048, 2048], P('grp', ('sp', 'tp')), parts along dimension 0
- final_state: float32 [2, 65536], P('grp', ('sp', 'tp')), parts along dimension 0
There are 2 independent parts, one for each index of `grp`. A program takes and returns all parts, laid end to end along the dimension named above; an argument that names none is the same for every part. Nothing has to cross between parts.
Inputs may be any that keep to these rules, and one draw needn't show every extreme that they name: `extra_decay`: no entry is positive.
All inputs are finite; a program needn't handle non-finite values.
Results may differ from a plain program's by a relative error of at most 0.014.
Values may be sent and summed in bfloat16 or wider, within the bound.
A program may use at most 128 MiB of HBM per device.

v0:
```python
import jax
import jax.numpy as jnp
from jax import lax
from jax.sharding import PartitionSpec as P

HEADS = 16
HEAD = 64
BLOCK = 64
EPSILON = 1e-05


def carried_in(value, axis, combine, identity):
    peers, mine = (lax.axis_size(axis), lax.axis_index(axis))
    everything = jax.tree.map(
        lambda part, kind: lax.all_gather(part.astype(kind), axis),
        value,
        (jnp.bfloat16, jnp.bfloat16),
    )
    start = jax.tree.map(
        lambda part, zero: jnp.broadcast_to(jnp.asarray(zero, part.dtype), part.shape),
        value,
        identity,
    )

    def step(k, before):
        reached = k < mine
        new = combine(
            before, jax.tree.map(lambda part, own: part[k].astype(own.dtype), everything, value)
        )
        return jax.tree.map(lambda a, b: jnp.where(reached, a, b), new, before)

    return lax.fori_loop(0, peers, step, start)


def broadcast(block, axis, source):
    block = jnp.where(lax.axis_index(axis) == source, block, jnp.zeros_like(block))
    return lax.psum(block, axis)


def layer_normed(tokens, norm_gain):
    values = tokens.astype(jnp.float32)
    center = values - jnp.mean(values, axis=-1, keepdims=True)
    spread = jnp.mean(center * center, axis=-1, keepdims=True)
    return (center * lax.rsqrt(spread + EPSILON) * norm_gain.astype(jnp.float32)).astype(
        jnp.bfloat16
    )


def gate_terms(query_sum, forget_sum, input_sum, floor_gap, extra_decay):
    query_raw = query_sum.astype(jnp.bfloat16)
    forget_raw = forget_sum.astype(jnp.bfloat16)
    input_raw = input_sum.astype(jnp.bfloat16)
    forget_pre = forget_raw.astype(jnp.float32)
    split_shape = forget_pre.shape[:-1] + (HEADS, HEAD)
    log_keep = jnp.logaddexp(
        jnp.log1p(-floor_gap), jnp.log(floor_gap) + jax.nn.log_sigmoid(forget_pre)
    )
    log_keep = log_keep.reshape(split_shape) + extra_decay[..., None]
    key_gate = (floor_gap * jax.nn.sigmoid(-forget_pre)).reshape(split_shape)
    query = jax.nn.silu(query_raw.astype(jnp.float32)).reshape(split_shape)
    values = input_raw.astype(jnp.float32).reshape(split_shape)
    return (query, key_gate, values, log_keep)


def block_pass(query, key_gate, values, log_keep):
    highest = lax.Precision.HIGHEST
    cumul = jnp.cumsum(log_keep, axis=2)
    q_decayed = query * jnp.exp(cumul)
    key_decayed = key_gate * jnp.exp(-cumul)
    causal = lax.broadcasted_iota(jnp.int32, (BLOCK, BLOCK), 0) >= lax.broadcasted_iota(
        jnp.int32, (BLOCK, BLOCK), 1
    )
    scores = jnp.einsum("snthd,snuhd->snhtu", q_decayed, key_decayed, precision=highest)
    scores = jnp.where(causal, scores, 0.0)
    within = jnp.einsum("snhtu,snuhe->snthe", scores, values, precision=highest)
    totals = cumul[:, :, -1]
    k_tail = key_gate * jnp.exp(totals[:, :, None] - cumul)
    block_state = jnp.einsum("snthd,snthe->snhde", k_tail, values, precision=highest)
    return (q_decayed, within, totals, block_state)


def linked_advance(earlier, later):
    return (earlier[0] + later[0], jnp.exp(later[0])[..., None] * earlier[1] + later[1])


def read_out(q_global, leading_logarithm, prefix_state, init_part):
    carried = jnp.exp(leading_logarithm)[..., None] * init_part + prefix_state
    added = jnp.einsum("snthd,shde->snthe", q_global, carried, precision=lax.Precision.HIGHEST)
    return (carried, added)


def body(
    tokens,
    norm_gain,
    w_query,
    w_forget,
    w_input,
    floor_gap,
    extra_decay,
    init_state,
    head_norm_gain,
    w_output,
):
    normed = layer_normed(tokens, norm_gain)
    seqs, span = (tokens.shape[0], tokens.shape[1])

    def add_rows(piece):
        return jnp.dot(normed, piece, preferred_element_type=jnp.float32)

    query_sum = add_rows(lax.all_gather(w_query, "sp", axis=0, tiled=True))
    forget_sum = add_rows(lax.all_gather(w_forget, "sp", axis=0, tiled=True))
    input_sum = add_rows(lax.all_gather(w_input, "sp", axis=0, tiled=True))
    query, key_gate, values, log_keep = gate_terms(
        query_sum, forget_sum, input_sum, floor_gap, extra_decay
    )
    blocks = span // BLOCK
    blocked = (seqs, blocks, BLOCK, HEADS, HEAD)
    q_decayed, within, totals, block_state = block_pass(
        query.reshape(blocked),
        key_gate.reshape(blocked),
        values.reshape(blocked),
        log_keep.reshape(blocked),
    )
    running_state = jnp.zeros((seqs, HEADS, HEAD, HEAD), jnp.float32)
    running_log = jnp.zeros((seqs, HEADS, HEAD), jnp.float32)
    entering_list = []
    offset_list = []
    for number in range(blocks):
        entering_list.append(running_state)
        offset_list.append(running_log)
        running_state = (
            jnp.exp(totals[:, number])[..., None] * running_state + block_state[:, number]
        )
        running_log = running_log + totals[:, number]
    entering = jnp.stack(entering_list, axis=1)
    offsets = jnp.stack(offset_list, axis=1)
    local_out = within + jnp.einsum(
        "snthd,snhde->snthe", q_decayed, entering, precision=lax.Precision.HIGHEST
    )
    q_global = q_decayed * jnp.exp(offsets[:, :, None])
    leading_logarithm, prefix_state = carried_in(
        (running_log, running_state),
        ("sp", "tp"),
        linked_advance,
        (jnp.zeros_like(running_log), jnp.zeros_like(running_state)),
    )
    carried, added = read_out(q_global, leading_logarithm, prefix_state, init_state)
    flat_total = HEADS * HEAD * HEAD
    piece_count = flat_total // lax.axis_size(("sp", "tp"))
    piece_start = lax.axis_index(("sp", "tp")) * piece_count
    after_state = (jnp.exp(running_log)[..., None] * carried + running_state).reshape(
        seqs, flat_total
    )
    whole_state = broadcast(
        after_state.astype(jnp.bfloat16), ("sp", "tp"), lax.axis_size(("sp", "tp")) - 1
    ).astype(after_state.dtype)
    final_state = lax.dynamic_slice_in_dim(whole_state, piece_start, piece_count, 1)
    recurrent = (local_out + added).reshape(seqs, span, HEADS, HEAD)
    average_power = jnp.mean(recurrent * recurrent, axis=-1, keepdims=True)
    scaled = (
        recurrent
        * lax.rsqrt(average_power + EPSILON)
        * head_norm_gain.astype(jnp.float32).reshape(HEADS, HEAD)
    )
    gated = scaled.reshape(seqs, span, HEADS * HEAD).astype(jnp.bfloat16)
    mixed = jnp.dot(
        gated,
        lax.all_gather(w_output, "sp", axis=1, tiled=True),
        preferred_element_type=jnp.float32,
    ).astype(jnp.bfloat16)
    return (mixed, final_state)


def solution(mesh):
    placed = (
        P("grp", ("sp", "tp"), None),
        P(),
        P("sp", None),
        P("sp", None),
        P("sp", None),
        P(),
        P("grp", ("sp", "tp"), None),
        P("grp", None, None, None),
        P(),
        P(None, "sp"),
    )
    return jax.shard_map(
        body,
        mesh=mesh,
        in_specs=placed,
        out_specs=(P("grp", ("sp", "tp"), None), P("grp", ("sp", "tp"))),
        check_vma=False,
    )
```

profile of v0, /device:TPU:0, one launch (start us, length us, event | category | flops | bytes accessed | tf_op | source)
XLA Modules:
  0.0 493.7 jit_solution(17431788789680109495)
XLA Ops:
  7.2 0.7 all-gather.10.cloned.1.call-update
  8.0 0.7 all-gather.8.cloned.1.call-update
  8.7 0.7 all-gather.6.cloned.1.call-update
  9.5 0.7 convert_element_type.119
  10.1 0.8 copy.63
  10.9 1.2 convert_reduce_fusion
  12.1 1.3 fusion.9
  13.5 79.6 %all-gather.10.cloned.1.call-done = bf16[2048,1024]{1,0:T(8,128)(2,1)} async-done(((bf16[512,1024]{1,0:T(8,128)(2,1)}), bf16[2048,1024]{1,0:T(8,128)(2,1)}) %all-gather.10.cloned.1.call-update) | async-done | bytes 4194320 | tf_op jit(solution)/shard_map/all_gather | solution.py:111
  93.1 3.7 add_select_fusion.1
  97.1 1.3 reshape_reshape.8
  98.4 75.5 %all-gather.8.cloned.1.call-done = bf16[2048,1024]{1,0:T(8,128)(2,1)} async-done(((bf16[512,1024]{1,0:T(8,128)(2,1)}), bf16[2048,1024]{1,0:T(8,128)(2,1)}) %all-gather.8.cloned.1.call-update) | async-done | bytes 4194320 | tf_op jit(solution)/shard_map/all_gather | solution.py:110
  173.9 3.0 divide_multiply_fusion.1
  177.0 1.3 reshape_reshape.7
  178.7 76.1 %all-gather.6.cloned.1.call-done = bf16[2048,1024]{1,0:T(8,128)(2,1)} async-done(((bf16[512,1024]{1,0:T(8,128)(2,1)}), bf16[2048,1024]{1,0:T(8,128)(2,1)}) %all-gather.6.cloned.1.call-update) | async-done | bytes 4194320 | tf_op jit(solution)/shard_map/all_gather | solution.py:112
  254.8 2.9 convolution_convert_fusion.3
  258.1 3.3 fusion.18
  261.5 1.2 convolution_bitcast_fusion.1
  262.7 1.2 add_convert_fusion
  264.6 19.4 %all_gather.23 = bf16[16,1,16,64]{3,2,1,0:T(8,128)(2,1)S(1)} all-gather(bf16[1,1,16,64]{3,2,1,0:T(8,128)(2,1)S(1)} %get-tuple-element.162), channel_id=1, replica_groups=mesh['grp'=2,'sp'=4,'tp'=4] {'sp','tp'}, dimensions={0}, use_global_device_ids=true | all-gather | bytes 34816 | tf_op jit(solution)/shard_map/all_gather | solution.py:15
  284.0 3.6 convolution_select_fusion
  287.6 1.0 fusion.34
  288.6 3.1 fusion.3
  291.7 21.5 %all-gather.12.cloned.1.call-done = bf16[16,1,16,64,64]{4,3,2,1,0:T(8,128)(2,1)} async-done(((bf16[1,1,16,64,64]{4,3,2,1,0:T(8,128)(2,1)}), bf16[16,1,16,64,64]{4,3,2,1,0:T(8,128)(2,1)}) %all-gather.12.cloned.1.call-update) | async-done | bytes 2097168 | tf_op jit(solution)/shard_map/all_gather | solution.py:15
  313.2 22.0 %while.16 = (s32[]{:T(128)}, f32[1,16,64]{2,1,0:T(8,128)S(1)}, f32[1,16,64,64]{3,2,1,0:T(8,128)S(1)}, s32[]{:T(128)}, bf16[16,1,16,64]{3,2,1,0:T(8,128)(2,1)S(1)...) while((s32[]{:T(128)}, f32[1,16,64]{2,1,0:T(8,128)S(1)}, ...), condition=%wide.region_4.5_spmd.clone, body=%wide.region_3.4_spmd.clone.sunk | while | flops 332804 | bytes 675959 | solution.py:32
  313.3 1.4 fusion.53
  314.7 1.3 fusion.53
  316.1 1.3 fusion.53
  317.4 1.3 fusion.53
  318.8 1.3 fusion.53
  320.2 1.3 fusion.53
  321.6 1.3 fusion.53
  322.9 1.3 fusion.53
  324.3 1.3 fusion.53
  325.7 1.3 fusion.53
  327.1 1.3 fusion.53
  328.4 1.3 fusion.53
  329.8 1.3 fusion.53
  331.1 1.3 fusion.53
  332.5 1.3 fusion.53
  333.9 1.3 fusion.53
  335.2 0.7 fusion.37
  336.0 0.9 select_n.80
  336.8 5.6 %multiply_reduce_fusion = (f32[2,64,16]{1,2,0:T(8,128)S(1)}, f32[1,2,64,16,64]{2,4,3,1,0:T(8,128)}) fusion(f32[1,2,64,16,64]{2,4,3,1,0:T(8,128)} %fusion.3, f32[2,64,16,64]{3,2,1,0:T(8,128)S(1)} %copy-done, f32[1,16,64,64]{3,2,1,0:T(8,128)S(1)} %get-tuple-element.113, f32[1,16,64,64]{3,2,1,0:T(8,128)S(1)} %copy-done.3, ...), kind=kOutput, calls=%fused_computation.39 | convolution fusion | flops 101185536 | bytes 2109440 | tf_op jit(solution)/shard_map/snthd,shde->snthe/dot_general | solution.py:88
  342.4 1.7 copy.56
  344.9 49.1 %all-gather.14.cloned.1.call-done = bf16[1024,2048]{1,0:T(8,128)(2,1)} async-done(((bf16[1024,512]{1,0:T(8,128)(2,1)}), bf16[1024,2048]{1,0:T(8,128)(2,1)}) %all-gather.14.cloned.1.call-update) | async-done | bytes 4194320 | tf_op jit(solution)/shard_map/all_gather | solution.py:168
  394.0 3.7 fusion.2
  397.7 87.8 %all-reduce.4.cloned.1.call-done = bf16[1,65536]{1,0:T(2,128)(2,1)} async-done(((bf16[1,65536]{1,0:T(2,128)(2,1)}), bf16[1,65536]{1,0:T(2,128)(2,1)}) %all-reduce.4.cloned.1.call-update) | async-done | bytes 131088 | tf_op jit(solution)/shard_map/psum | solution.py:37
  485.5 1.3 dynamic-slice_convert_fusion
  (73 shorter events, 3.0 us)
Async XLA Ops:
  7.2 86.0 %copy-start.2 = (bf16[1,128,2048]{2,1,0:T(8,128)(2,1)S(1)}, bf16[1,128,2048]{2,1,0:T(8,128)(2,1)}, u32[]{:S(2)}) copy-start(bf16[1,128,2048]{2,1,0:T(8,128)(2,1)} %param.12) | copy-start | bytes 1572868
  7.2 6.3 %copy-start.4 = (f32[1024]{0:T(1024)S(1)}, f32[1024]{0:T(1024)}, u32[]{:S(2)}) copy-start(f32[1024]{0:T(1024)} %param.17) | copy-start | bytes 12292
  7.2 85.9 %all-gather.10.cloned.1.call-start = ((), (), s32[]{:S(2)}) async-start(), calls=%async_computation.2 | async-start | bytes 5242880 | tf_op jit(solution)/shard_map/all_gather | solution.py:111
  7.9 166.0 %all-gather.8.cloned.1.call-start = ((), (), s32[]{:S(2)}) async-start(), calls=%async_computation.1 | async-start | bytes 5242880 | tf_op jit(solution)/shard_map/all_gather | solution.py:110
  8.7 246.1 %all-gather.6.cloned.1.call-start = ((), (), s32[]{:S(2)}) async-start(), calls=%async_computation | async-start | bytes 5242880 | tf_op jit(solution)/shard_map/all_gather | solution.py:112
  9.4 303.8 %all-gather.12.cloned.1.call-start = ((), (), s32[]{:S(2)}) async-start(), calls=%async_computation.3 | async-start | bytes 4456448 | tf_op jit(solution)/shard_map/all_gather | solution.py:15
  261.5 3.1 copy-start.5
  263.9 130.1 %all-gather.14.cloned.1.call-start = ((), (), s32[]{:S(2)}) async-start(), calls=%async_computation.4 | async-start | bytes 5242880 | tf_op jit(solution)/shard_map/all_gather | solution.py:168
  264.5 221.0 %all-reduce.4.cloned.1.call-start = ((), (), s32[]{:S(2)}) async-start(), calls=%async_computation.5 | async-start | bytes 524288 | tf_op jit(solution)/shard_map/psum | solution.py:37
  264.6 24.0 %copy-start.1 = (f32[1,1,16,64,64]{4,3,2,1,0:T(8,128)S(1)}, f32[1,1,16,64,64]{4,3,2,1,0:T(8,128)}, u32[]{:S(2)}) copy-start(f32[1,1,16,64,64]{4,3,2,1,0:T(8,128)} %get-tuple-element.148) | copy-start | bytes 786436
  291.7 43.5 %copy-start.3 = (f32[1,16,64,64]{3,2,1,0:T(8,128)S(1)}, f32[1,16,64,64]{3,2,1,0:T(8,128)}, u32[]{:S(2)}) copy-start(f32[1,16,64,64]{3,2,1,0:T(8,128)} %param.19) | copy-start | bytes 786436
  313.2 23.6 %copy-start = (f32[2,64,16,64]{3,2,1,0:T(8,128)S(1)}, f32[2,64,16,64]{3,2,1,0:T(8,128)}, u32[]{:S(2)}) copy-start(f32[2,64,16,64]{3,2,1,0:T(8,128)} %get-tuple-element.153) | copy-start | bytes 1572868
Sparse Core Ops, SparseCore 0:
  9.6 83.5 all-gather.9
  94.7 79.2 all-gather.7
  175.5 79.2 all-gather.5
  264.0 49.1 all-gather.11
  314.7 79.2 all-gather.13
  397.2 88.2 all-reduce.3
where the time goes:
time: 495 us; the launch traced here: 494 us
  waiting for transfers between devices  392 us (79%)
  other arithmetic  31.6 us (6%)
  matrix products  27.9 us (6%)
  blocking collectives  19.4 us (4%)
  between operations  14.3 us (3%)
  local copies, waits for them, and re-layouts  7.27 us (1%)
    psum x1, waiting for transfers between devices, broadcast(): return lax.psum(block, axis)  87.8 us
    all_gather x1, waiting for transfers between devices, body(): forget_sum = add_rows(lax.all_gather(w_forget, 'sp', axis=0, tiled=True))  79.6 us
    all_gather x1, waiting for transfers between devices, body(): input_sum = add_rows(lax.all_gather(w_input, 'sp', axis=0, tiled=True))  76.1 us
    all_gather x1, waiting for transfers between devices, body(): query_sum = add_rows(lax.all_gather(w_query, 'sp', axis=0, tiled=True))  75.5 us
    all_gather x1, waiting for transfers between devices, body(): lax.all_gather(w_output, 'sp', axis=1, tiled=True)  49.1 us
    all_gather x1, waiting for transfers between devices, carried_in(): lax.all_gather(part.astype(kind), axis)  21.5 us
    select_n x32, other arithmetic, step(): return jax.tree.map(lambda a, b: jnp.where(reached, a, b), new, before)  21.1 us
    all_gather x1, blocking collectives, carried_in(): lax.all_gather(part.astype(kind), axis)  19.4 us
  transfers between devices with their start and end apart: 6, of which 6 were waited for; matrix products, arithmetic and copies ran while one was open for 11% of the time, Pallas kernels for 0%

commit v1 on v0

--- a/solution.py
+++ b/solution.py
@@ -34,7 +34,12 @@
 
 def broadcast(block, axis, source):
     block = jnp.where(lax.axis_index(axis) == source, block, jnp.zeros_like(block))
-    return lax.psum(block, axis)
+
+    def _note_point(local_values):
+        x_new = jnp.sum(jax.lax.all_gather(local_values, axis), axis=0)
+        return x_new
+
+    return _note_point(block)
 
 
 def layer_normed(tokens, norm_gain):

time: 495 us -> 459 us (0.927)
  waiting for transfers between devices: 392 us -> 354 us
  other arithmetic: 31.6 us -> 37.9 us
    psum x1 -> x0, waiting for transfers between devices: 87.8 us -> none  [broadcast(): return lax.psum(block, axis)]
    all_gather x0 -> x1, waiting for transfers between devices: none -> 47.2 us  [_note_point(): x_new = jnp.sum(jax.lax.all_gather(local_values, axis), axis=0)]
    all_gather x1, waiting for transfers between devices: 21.5 us -> 29.4 us  [carried_in(): lax.all_gather(part.astype(kind), axis)]
    reduce_sum x0 -> x1, other arithmetic: none -> 5.99 us  [_note_point(): x_new = jnp.sum(jax.lax.all_gather(local_values, axis), axis=0)]
    all_gather x1, waiting for transfers between devices: 49.1 us -> 43.5 us  [body(): lax.all_gather(w_output, 'sp', axis=1, tiled=True)]
  transfers between devices with their start and end apart: 6 -> 6, of which waited for: 6 -> 6; matrix products, arithmetic and copies ran while one was open for 11% -> 12% of each run, Pallas kernels for 0% -> 0%
where the time goes in v1:
time: 459 us; the launch traced here: 458 us
  waiting for transfers between devices  354 us (77%)
  other arithmetic  37.9 us (8%)
  matrix products  25.8 us (6%)
  blocking collectives  19.2 us (4%)
  between operations  14.4 us (3%)
  local copies, waits for them, and re-layouts  6.09 us (1%)
    all_gather x1, waiting for transfers between devices, body(): forget_sum = add_rows(lax.all_gather(w_forget, 'sp', axis=0, tiled=True))  79.6 us
    all_gather x1, waiting for transfers between devices, body(): input_sum = add_rows(lax.all_gather(w_input, 'sp', axis=0, tiled=True))  76.1 us
    all_gather x1, waiting for transfers between devices, body(): query_sum = add_rows(lax.all_gather(w_query, 'sp', axis=0, tiled=True))  75.5 us
    all_gather x1, waiting for transfers between devices, _note_point(): x_new = jnp.sum(jax.lax.all_gather(local_values, axis), axis=0)  47.2 us
    all_gather x1, waiting for transfers between devices, body(): lax.all_gather(w_output, 'sp', axis=1, tiled=True)  43.5 us
    all_gather x1, waiting for transfers between devices, carried_in(): lax.all_gather(part.astype(kind), axis)  29.4 us
    select_n x32, other arithmetic, step(): return jax.tree.map(lambda a, b: jnp.where(reached, a, b), new, before)  21 us
    all_gather x1, blocking collectives, carried_in(): lax.all_gather(part.astype(kind), axis)  19.2 us
  transfers between devices with their start and end apart: 6, of which 6 were waited for; matrix products, arithmetic and copies ran while one was open for 12% of the time, Pallas kernels for 0%

profile of v1, /device:TPU:0, one launch (start us, length us, event | category | flops | bytes accessed | tf_op | source)
XLA Modules:
  0.0 458.2 jit_solution(1221731218433785744)
XLA Ops:
  7.2 0.7 all-gather.11.cloned.1.call-update
  8.0 0.7 all-gather.9.cloned.1.call-update
  8.7 0.7 all-gather.7.cloned.1.call-update
  9.5 0.7 convert_element_type.131
  10.1 0.8 copy.63
  10.9 1.2 convert_reduce_fusion
  12.1 1.3 fusion.9
  13.5 79.6 %all-gather.11.cloned.1.call-done = bf16[2048,1024]{1,0:T(8,128)(2,1)} async-done(((bf16[512,1024]{1,0:T(8,128)(2,1)}), bf16[2048,1024]{1,0:T(8,128)(2,1)}) %all-gather.11.cloned.1.call-update) | async-done | bytes 4194320 | tf_op jit(solution)/shard_map/all_gather | solution.py:116
  93.1 3.7 add_select_fusion.1
  97.1 1.3 reshape_reshape.8
  98.4 75.5 %all-gather.9.cloned.1.call-done = bf16[2048,1024]{1,0:T(8,128)(2,1)} async-done(((bf16[512,1024]{1,0:T(8,128)(2,1)}), bf16[2048,1024]{1,0:T(8,128)(2,1)}) %all-gather.9.cloned.1.call-update) | async-done | bytes 4194320 | tf_op jit(solution)/shard_map/all_gather | solution.py:115
  173.9 3.0 divide_multiply_fusion.1
  177.0 1.3 reshape_reshape.7
  178.7 76.1 %all-gather.7.cloned.1.call-done = bf16[2048,1024]{1,0:T(8,128)(2,1)} async-done(((bf16[512,1024]{1,0:T(8,128)(2,1)}), bf16[2048,1024]{1,0:T(8,128)(2,1)}) %all-gather.7.cloned.1.call-update) | async-done | bytes 4194320 | tf_op jit(solution)/shard_map/all_gather | solution.py:117
  254.8 2.9 convolution_convert_fusion.3
  258.1 3.3 fusion.18
  261.5 1.2 convolution_bitcast_fusion.1
  262.6 1.2 add_convert_fusion
  264.6 19.2 %all_gather.27 = bf16[16,1,16,64]{3,2,1,0:T(8,128)(2,1)S(1)} all-gather(bf16[1,1,16,64]{3,2,1,0:T(8,128)(2,1)S(1)} %get-tuple-element.162), channel_id=1, replica_groups=mesh['grp'=2,'sp'=4,'tp'=4] {'sp','tp'}, dimensions={0}, use_global_device_ids=true | all-gather | bytes 34816 | tf_op jit(solution)/shard_map/all_gather | solution.py:15
  283.7 29.4 %all-gather.13.cloned.1.call-done = bf16[16,1,16,64,64]{4,3,2,1,0:T(8,128)(2,1)} async-done(((bf16[1,1,16,64,64]{4,3,2,1,0:T(8,128)(2,1)}), bf16[16,1,16,64,64]{4,3,2,1,0:T(8,128)(2,1)}) %all-gather.13.cloned.1.call-update) | async-done | bytes 2097168 | tf_op jit(solution)/shard_map/all_gather | solution.py:15
  313.1 21.9 %while.16 = (s32[]{:T(128)}, f32[1,16,64]{2,1,0:T(8,128)S(1)}, f32[1,16,64,64]{3,2,1,0:T(8,128)S(1)}, s32[]{:T(128)}, bf16[16,1,16,64]{3,2,1,0:T(8,128)(2,1)S(1)...) while((s32[]{:T(128)}, f32[1,16,64]{2,1,0:T(8,128)S(1)}, ...), condition=%wide.region_4.5_spmd.clone, body=%wide.region_3.4_spmd.clone.sunk | while | flops 332804 | bytes 675959 | solution.py:32
  313.1 1.3 fusion.53
  314.5 1.3 fusion.53
  315.9 1.3 fusion.53
  317.2 1.3 fusion.53
  318.6 1.3 fusion.53
  320.0 1.3 fusion.53
  321.4 1.3 fusion.53
  322.7 1.3 fusion.53
  324.1 1.3 fusion.53
  325.5 1.3 fusion.53
  326.9 1.3 fusion.53
  328.2 1.3 fusion.53
  329.6 1.3 fusion.53
  330.9 1.3 fusion.53
  332.3 1.3 fusion.53
  333.7 1.3 fusion.53
  335.0 1.9 fusion.37
  336.9 0.9 select_n.81
  337.9 3.7 convolution_select_fusion
  341.6 1.0 fusion.34
  342.6 3.1 fusion.3
  345.8 3.4 multiply_reduce_fusion
  350.3 43.5 %all-gather.15.cloned.1.call-done = bf16[1024,2048]{1,0:T(8,128)(2,1)} async-done(((bf16[1024,512]{1,0:T(8,128)(2,1)}), bf16[1024,2048]{1,0:T(8,128)(2,1)}) %all-gather.15.cloned.1.call-update) | async-done | bytes 4194320 | tf_op jit(solution)/shard_map/all_gather | solution.py:173
  393.8 3.7 fusion.2
  397.6 47.2 %all-gather.17.cloned.1.call-done = bf16[16,1,65536]{2,1,0:T(2,128)(2,1)} async-done(((bf16[1,1,65536]{2,1,0:T(2,128)(2,1)}), bf16[16,1,65536]{2,1,0:T(2,128)(2,1)}) %all-gather.17.cloned.1.call-update) | async-done | bytes 2097168 | tf_op jit(solution)/shard_map/all_gather | solution.py:39
  444.8 6.0 %reduce_sum.42 = bf16[65536]{0:T(1024)(128)(2,1)S(1)} reduce(bf16[16,1,65536]{2,1,0:T(2,128)(2,1)} %all-gather.17.cloned.1.call-done, bf16[]{:T(256)} %constant.65.clone.1), dimensions={0,1}, to_apply=%region_6.7 | reduce | flops 983040 | bytes 2228226 | tf_op jit(solution)/shard_map/reduce_sum | solution.py:39
  450.8 0.6 dynamic-slice_convert_fusion
  (72 shorter events, 3.5 us)
Async XLA Ops:
  7.2 86.0 %copy-start.1 = (bf16[1,128,2048]{2,1,0:T(8,128)(2,1)S(1)}, bf16[1,128,2048]{2,1,0:T(8,128)(2,1)}, u32[]{:S(2)}) copy-start(bf16[1,128,2048]{2,1,0:T(8,128)(2,1)} %param.12) | copy-start | bytes 1572868
  7.2 6.3 %copy-start.3 = (f32[1024]{0:T(1024)S(1)}, f32[1024]{0:T(1024)}, u32[]{:S(2)}) copy-start(f32[1024]{0:T(1024)} %param.17) | copy-start | bytes 12292
  7.2 85.9 %all-gather.11.cloned.1.call-start = ((), (), s32[]{:S(2)}) async-start(), calls=%async_computation.2 | async-start | bytes 5242880 | tf_op jit(solution)/shard_map/all_gather | solution.py:116
  7.9 166.0 %all-gather.9.cloned.1.call-start = ((), (), s32[]{:S(2)}) async-start(), calls=%async_computation.1 | async-start | bytes 5242880 | tf_op jit(solution)/shard_map/all_gather | solution.py:115
  8.7 246.1 %all-gather.7.cloned.1.call-start = ((), (), s32[]{:S(2)}) async-start(), calls=%async_computation | async-start | bytes 5242880 | tf_op jit(solution)/shard_map/all_gather | solution.py:117
  9.4 303.7 %all-gather.13.cloned.1.call-start = ((), (), s32[]{:S(2)}) async-start(), calls=%async_computation.3 | async-start | bytes 4456448 | tf_op jit(solution)/shard_map/all_gather | solution.py:15
  263.9 130.0 %all-gather.15.cloned.1.call-start = ((), (), s32[]{:S(2)}) async-start(), calls=%async_computation.4 | async-start | bytes 5242880 | tf_op jit(solution)/shard_map/all_gather | solution.py:173
  264.5 180.3 %all-gather.17.cloned.1.call-start = ((), (), s32[]{:S(2)}) async-start(), calls=%async_computation.5 | async-start | bytes 4456448 | tf_op jit(solution)/shard_map/all_gather | solution.py:39
  313.1 24.7 %copy-start.4 = (bf16[1024]{0:T(1024)(128)(2,1)S(1)}, bf16[1024]{0:T(1024)(128)(2,1)}, u32[]{:S(2)}) copy-start(bf16[1024]{0:T(1024)(128)(2,1)} %param.20) | copy-start | bytes 6148
  337.8 7.9 %copy-start = (f32[2,64,16,64]{3,2,1,0:T(8,128)S(1)}, f32[2,64,16,64]{3,2,1,0:T(8,128)}, u32[]{:S(2)}) copy-start(f32[2,64,16,64]{3,2,1,0:T(8,128)} %get-tuple-element.153) | copy-start | bytes 1572868
  337.9 7.9 %copy-start.2 = (f32[1,16,64,64]{3,2,1,0:T(8,128)S(1)}, f32[1,16,64,64]{3,2,1,0:T(8,128)}, u32[]{:S(2)}) copy-start(f32[1,16,64,64]{3,2,1,0:T(8,128)} %param.19) | copy-start | bytes 786436
Sparse Core Ops, SparseCore 0:
  9.6 83.5 all-gather.10
  94.7 79.2 all-gather.8
  175.5 79.2 all-gather.6
  264.0 49.0 all-gather.12
  314.5 79.2 all-gather.14
  395.9 48.8 all-gather.16
